TPU v7x, 512 devices: a whole 4x4x16 slice. The times are simulated.
512 devices in a mesh: kv: 16 (over y, x), tp: 32 (over z, core).
Axes of the slice: x: 4, y: 4, z: 16, core: 2. Of those that a mesh axis runs over, the one named last changes fastest.
Arguments:
- tokens: bfloat16 [2048, 2048], P('tp', 'kv'), may hold values from -16 to 16
- lengths: int32 [2048], P('tp'), may hold values from 1 to 8192, 2097152 in all
- query_weight: bfloat16 [2048, 1024], P(None, 'kv'), may hold values from -0.125 to 0.125
- key_weight: bfloat16 [2048, 1024], P(None, 'kv'), may hold values from -0.125 to 0.125
- value_weight: bfloat16 [2048, 1024], P(None, 'kv'), may hold values from -0.125 to 0.125
- gate_weight: bfloat16 [2048, 1024], P(None, 'kv'), may hold values from -0.125 to 0.125
- output_weight: bfloat16 [1024, 2048], P('kv'), may hold values from -0.1875 to 0.1875
- mixer_gain: float32 [2048], replicated, may hold values from 0.1 to 1.9
- group_gain: float32 [1024], P('kv'), may hold values from 0.1 to 1.9
- channel_gain: float32 [2048], P('kv'), may hold values from 0.1 to 1.9
- up_weight: bfloat16 [2048, 8192], P('kv', 'tp'), may hold values from -0.125 to 0.125
- down_weight: bfloat16 [8192, 2048], P('tp', 'kv'), may hold values from -0.0625 to 0.0625
- memory_state: float32 [2048, 16, 64, 64], P('tp', 'kv'), may hold values from -0.6 to 0.6
Outputs:
- mixed: bfloat16 [2048, 2048], P('tp', 'kv')
- new_state: float32 [2048, 16, 64, 64], P('tp', 'kv')
All inputs are finite; a program needn't handle non-finite values. No bound on the sum of `lengths` on one device may be relied on, other than what follows from the above.
Results may differ from a plain program's by a relative error of at most 0.012.
Values may be sent and summed in bfloat16 or wider, within the bound.
No kernel may reach another device: no remote copies, remote signals or barrier semaphores. Data moves between devices by JAX's collectives and lax.ppermute only.
A program may use at most 64 MiB of HBM per device.

v0:
```python
import math

import jax
import jax.numpy as jnp
from jax import lax
from jax.sharding import PartitionSpec as P

D = 2048
HEADS = 16
HEAD_DIM = 64


EPS = 1e-06
THETA = 10000.0


def sent_to_all(value, axis):
    copies = jnp.broadcast_to(value, (lax.axis_size(axis), *value.shape))
    return lax.all_to_all(copies, axis, split_axis=0, concat_axis=0, tiled=True)


def joined_along(blocks, dim):
    dims = list(blocks.shape[1:])
    dims[dim] *= blocks.shape[0]
    return jnp.moveaxis(blocks, 0, dim).reshape(dims)


def collect(value, axis, dim):
    blocks = sent_to_all(value, axis)
    return joined_along(blocks, dim)


def cut_along(value, dim, size):
    dims = value.shape
    blocks = value.reshape(*dims[:dim], size, dims[dim] // size, *dims[dim + 1 :])
    return jnp.moveaxis(blocks, dim, 0)


def sent_and_summed(value, axis, dim):
    size = lax.axis_size(axis)
    blocks = lax.all_to_all(cut_along(value, dim, size), axis, 0, 0, tiled=True)
    return jnp.sum(blocks, axis=0)


def summed_on_arrival(value, axis, dim):
    blocks = cut_along(value, dim, lax.axis_size(axis))
    arrived = lax.all_to_all(blocks, axis, split_axis=0, concat_axis=0, tiled=True)
    return arrived.astype(jnp.float32).sum(axis=0)


def side_by_side(arrays, axis, dim, along):
    widths = [math.prod(a.shape[along:]) for a in arrays]
    both = jnp.concatenate(
        [a.reshape(*a.shape[:along], w) for a, w in zip(arrays, widths)], axis=along
    )
    filled = summed_on_arrival(both, axis, dim)
    blocks = jnp.split(filled, [sum(widths[:k]) for k in range(1, len(widths))], axis=along)
    return tuple(
        (b.reshape(*filled.shape[:along], *a.shape[along:]) for a, b in zip(arrays, blocks))
    )


def rotate(vectors, position):
    breadth = vectors.shape[-1]
    middle = breadth // 2
    inverse = THETA ** (-jnp.arange(middle, dtype=jnp.float32) * 2.0 / breadth)
    angles = position.astype(jnp.float32)[:, None] * inverse[None, :]
    cosine = jnp.cos(angles)[:, None, :]
    sine_part = jnp.sin(angles)[:, None, :]
    former = vectors[..., :middle]
    latter = vectors[..., middle:]
    return jnp.concatenate(
        [former * cosine - latter * sine_part, former * sine_part + latter * cosine], axis=-1
    )


def on_device(
    tokens,
    lengths,
    query_weight,
    key_weight,
    value_weight,
    gate_weight,
    output_weight,
    mixer_gain,
    group_gain,
    channel_gain,
    up_weight,
    down_weight,
    memory_state,
):
    whole_rows = collect(tokens, "kv", 1)
    widened = whole_rows.astype(jnp.float32)
    normed = (
        widened * lax.rsqrt(jnp.mean(widened * widened, axis=1, keepdims=True) + EPS) * mixer_gain
    ).astype(jnp.bfloat16)
    served = tokens.shape[0]
    local_heads = query_weight.shape[1] // HEAD_DIM

    def project(weight):
        return jnp.dot(normed, weight, preferred_element_type=jnp.float32).reshape(
            served, local_heads, HEAD_DIM
        )

    queries = rotate(project(query_weight), lengths)
    keys_new = rotate(project(key_weight), lengths) * HEAD_DIM ** (-0.5)
    values_new = project(value_weight)
    gating = jnp.dot(normed, gate_weight, preferred_element_type=jnp.float32)
    head_ids = (lax.axis_index("kv") * local_heads + jnp.arange(local_heads)).astype(jnp.float32)
    decays = 1.0 - 2.0 ** (-5.0 - 5.0 * head_ids / (HEADS - 1))
    new_state = (
        decays[None, :, None, None] * memory_state
        + keys_new[:, :, :, None] * values_new[:, :, None, :]
    )
    readout = jnp.einsum("bhkv,bhk->bhv", new_state, queries, precision=lax.Precision.HIGHEST)
    grouped = readout * lax.rsqrt(jnp.mean(readout * readout, axis=-1, keepdims=True) + EPS)
    grouped = grouped * group_gain.reshape(local_heads, HEAD_DIM)
    merged = (grouped.reshape(served, local_heads * HEAD_DIM) * jax.nn.silu(gating)).astype(
        jnp.bfloat16
    )
    partial_value = jnp.dot(merged, output_weight, preferred_element_type=jnp.float32)
    mixed_part = sent_and_summed(partial_value, "kv", 1)
    after_mixer = (tokens.astype(jnp.float32) + mixed_part).astype(jnp.bfloat16)
    all_rows = collect(after_mixer, "tp", 0)
    residual = all_rows.astype(jnp.float32)
    squares = jnp.sum(residual * residual, axis=1)
    scaled = (residual * channel_gain).astype(jnp.bfloat16)
    raised_part = jnp.dot(scaled, up_weight, preferred_element_type=jnp.float32)
    raised, totals = side_by_side(
        (raised_part.astype(jnp.bfloat16), squares.astype(jnp.bfloat16)), "kv", 0, 1
    )
    factor = lax.rsqrt(totals / D + EPS)
    shared = jnp.square(jax.nn.relu(raised * factor[:, None])).astype(jnp.bfloat16)
    hidden = collect(shared, "kv", 0)
    lowered = sent_and_summed(
        jnp.dot(hidden, down_weight, preferred_element_type=jnp.float32), "tp", 0
    )
    mixed = (after_mixer.astype(jnp.float32) + lowered).astype(jnp.bfloat16)
    return (mixed, new_state)


def solution(mesh):
    return jax.shard_map(
        on_device,
        mesh=mesh,
        in_specs=(
            P("tp", "kv"),
            P("tp"),
            P(None, "kv"),
            P(None, "kv"),
            P(None, "kv"),
            P(None, "kv"),
            P("kv", None),
            P(),
            P("kv"),
            P("kv"),
            P("kv", "tp"),
            P("tp", "kv"),
            P("tp", "kv", None, None),
        ),
        out_specs=(P("tp", "kv"), P("tp", "kv", None, None)),
        check_vma=False,
    )
```

profile of v0, /device:TPU:1, one launch (start us, length us, event | category | flops | bytes accessed | tf_op | source)
XLA Modules:
  0.0 192.7 jit_solution(16598334162448619993)
XLA Ops:
  0.6 0.0 copy-start
  0.7 1.5 broadcast_in_dim.6
  2.2 7.6 %all-to-all-start = ((bf16[16,64,128]{2,1,0:T(8,128)(2,1)}), bf16[16,64,128]{2,1,0:T(8,128)(2,1)S(1)}, u32[]{:S(2)}, u32[]{:S(2)}) async-start(bf16[16,64,128]{2,1,0:T(8,128)(2,1)} %broadcast_in_dim.6), calls=%async_computation | async-start | bytes 524288 | tf_op jit(solution)/shard_map/all_to_all | solution.py:19
  9.8 0.7 convert_element_type.81
  10.5 7.0 %all-to-all-done = bf16[16,64,128]{2,1,0:T(8,128)(2,1)S(1)} async-done(((bf16[16,64,128]{2,1,0:T(8,128)(2,1)}), bf16[16,64,128]{2,1,0:T(8,128)(2,1)S(1)}, u32[]{:S(2)}, u32[]{:S(2)}) %all-to-all-start) | async-done | bytes 262176 | tf_op jit(solution)/shard_map/all_to_all | solution.py:19
  17.5 0.2 fusion.3
  17.6 0.8 fusion.5
  18.5 1.2 convolution_bitcast_fusion.1
  19.7 0.2 fusion.28
  19.9 0.2 convolution_bitcast_fusion.2
  20.1 0.2 fusion.17
  20.3 0.1 copy.39
  20.4 0.1 copy.45
  20.5 1.9 %multiply_add_fusion = f32[64,1,64,64]{3,2,1,0:T(8,128)S(1)} fusion(f32[64,1,64,64]{3,2,1,0:T(8,128)} %param.25, f32[]{:T(128)S(6)} %sub.17, f32[64,64]{1,0:T(8,128)S(1)} %fusion.28, f32[64,64]{1,0:T(8,128)S(1)} %copy.39), kind=kLoop, calls=%fused_computation.4 | loop fusion | flops 786432 | bytes 2129924 | tf_op jit(solution)/shard_map/add | solution.py:112
  22.4 0.0 copy-start.1
  22.4 0.0 copy-start.4
  22.4 0.0 copy-start.8
  22.4 1.9 fusion
  24.4 0.1 multiply_reduce_fusion.1
  24.5 0.0 copy-done
  24.5 0.0 copy-done.4
  24.5 0.0 copy-done.8
  24.5 0.5 convolution_bitcast_fusion
  25.1 0.0 copy-start.9
  25.1 12.0 %all_to_all.30 = f32[16,64,128]{2,1,0:T(8,128)S(1)} all-to-all(f32[16,64,128]{2,1,0:T(8,128)S(1)} %bitcast.58), channel_id=1, replica_groups=mesh['kv'=16,'tp'=32] {'kv'}, dimensions={0} | all-to-all | bytes 1048576 | tf_op jit(solution)/shard_map/all_to_all | solution.py:41
  37.1 0.0 copy-done.7
  37.2 0.1 broadcast_in_dim.7
  37.3 51.9 %all_to_all.31 = bf16[32,64,128]{2,1,0:T(8,128)(2,1)S(1)} all-to-all(bf16[32,64,128]{2,1,0:T(8,128)(2,1)S(1)} %broadcast_in_dim.7), channel_id=1, replica_groups=mesh['kv'=16,'tp'=32] {'tp'}, dimensions={0} | all-to-all | bytes 1048576 | tf_op jit(solution)/shard_map/all_to_all | solution.py:19
  89.1 0.4 multiply_reduce_fusion
  89.5 0.1 convert_element_type.98
  89.6 0.0 copy-done.9
  89.6 0.1 fusion.2
  89.7 0.4 convolution_convert_fusion
  90.1 0.7 copy.41
  90.8 0.1 pad_maximum_fusion
  90.9 19.4 %all_to_all.32 = bf16[16,128,257]{1,2,0:T(8,128)(2,1)S(1)} all-to-all(bf16[16,128,257]{1,2,0:T(8,128)(2,1)S(1)} %pad_maximum_fusion), channel_id=1, replica_groups=mesh['kv'=16,'tp'=32] {'kv'}, dimensions={0} | all-to-all | bytes 2105344 | tf_op jit(solution)/shard_map/all_to_all | solution.py:47
  110.3 0.5 convert_reduce_fusion
  110.8 0.0 copy-start.6
  110.8 0.1 copy.48
  110.9 0.1 copy.49
  111.0 0.1 rsqrt_reduce_fusion
  111.2 0.1 multiply_convert_fusion
  111.3 0.1 broadcast_in_dim.8
  111.4 18.4 %all_to_all.33 = bf16[16,128,256]{2,1,0:T(8,128)(2,1)S(1)} all-to-all(bf16[16,128,256]{2,1,0:T(8,128)(2,1)S(1)} %broadcast_in_dim.8), channel_id=1, replica_groups=mesh['kv'=16,'tp'=32] {'kv'}, dimensions={0} | all-to-all | bytes 2097152 | tf_op jit(solution)/shard_map/all_to_all | solution.py:19
  129.8 0.4 fusion.6
  130.2 61.7 %all_to_all.34 = f32[32,64,128]{2,1,0:T(8,128)S(1)} all-to-all(f32[32,64,128]{2,1,0:T(8,128)S(1)} %fusion.6), channel_id=1, replica_groups=mesh['kv'=16,'tp'=32] {'tp'}, dimensions={0} | all-to-all | bytes 2097152 | tf_op jit(solution)/shard_map/all_to_all | solution.py:41
  192.0 0.1 reduce_sum.59
  192.1 0.6 add_convert_fusion
  (19 shorter events, 0.2 us)
Async XLA Ops:
  0.6 23.8 %copy-start = (bf16[64,2048]{1,0:T(8,128)(2,1)S(1)}, bf16[64,2048]{1,0:T(8,128)(2,1)}, u32[]{:S(2)}) copy-start(bf16[64,2048]{1,0:T(8,128)(2,1)} %param.19) | copy-start | bytes 786436
  0.6 19.0 %copy-start.2 = (bf16[2048,64]{0,1:T(8,128)(2,1)S(1)}, bf16[2048,64]{0,1:T(8,128)(2,1)}, u32[]{:S(2)}) copy-start(bf16[2048,64]{0,1:T(8,128)(2,1)} %param.17) | copy-start | bytes 786436
  0.7 19.2 %copy-start.3 = (bf16[2048,64]{0,1:T(8,128)(2,1)S(1)}, bf16[2048,64]{0,1:T(8,128)(2,1)}, u32[]{:S(2)}) copy-start(bf16[2048,64]{0,1:T(8,128)(2,1)} %param.16) | copy-start | bytes 786436
  2.2 15.3 %all-to-all-start = ((bf16[16,64,128]{2,1,0:T(8,128)(2,1)}), bf16[16,64,128]{2,1,0:T(8,128)(2,1)S(1)}, u32[]{:S(2)}, u32[]{:S(2)}) async-start(bf16[16,64,128]{2,1,0:T(8,128)(2,1)} %broadcast_in_dim.6), calls=%async_computation | async-start | bytes 524288 | tf_op jit(solution)/shard_map/all_to_all | solution.py:19
  22.4 2.7 %copy-start.1 = (f32[64,1,64,64]{3,2,1,0:T(8,128)}, f32[64,1,64,64]{3,2,1,0:T(8,128)S(1)}, u32[]{:S(2)}) copy-start(f32[64,1,64,64]{3,2,1,0:T(8,128)S(1)} %multiply_add_fusion) | copy-start | bytes 3145732
  22.4 2.1 %copy-start.4 = (bf16[2048,64]{0,1:T(8,128)(2,1)S(1)}, bf16[2048,64]{0,1:T(8,128)(2,1)}, u32[]{:S(2)}) copy-start(bf16[2048,64]{0,1:T(8,128)(2,1)} %param.18) | copy-start | bytes 786436
  22.4 2.1 %copy-start.8 = (f32[64]{0:T(128)S(1)}, f32[64]{0:T(128)}, u32[]{:S(2)}) copy-start(f32[64]{0:T(128)} %param.21) | copy-start | bytes 772
  24.3 12.8 %copy-start.7 = (bf16[64,128]{1,0:T(8,128)(2,1)S(1)}, bf16[64,128]{1,0:T(8,128)(2,1)}, u32[]{:S(2)}) copy-start(bf16[64,128]{1,0:T(8,128)(2,1)} %param.13) | copy-start | bytes 49156
  25.1 64.5 %copy-start.9 = (f32[128]{0:T(128)S(1)}, f32[128]{0:T(128)}, u32[]{:S(2)}) copy-start(f32[128]{0:T(128)} %param.22) | copy-start | bytes 1540
  37.1 52.6 %copy-start.5 = (bf16[128,256]{1,0:T(8,128)(2,1)S(1)}, bf16[128,256]{1,0:T(8,128)(2,1)}, u32[]{:S(2)}) copy-start(bf16[128,256]{1,0:T(8,128)(2,1)} %param.23) | copy-start | bytes 196612
  110.8 19.0 %copy-start.6 = (bf16[256,128]{1,0:T(8,128)(2,1)S(1)}, bf16[256,128]{1,0:T(8,128)(2,1)}, u32[]{:S(2)}) copy-start(bf16[256,128]{1,0:T(8,128)(2,1)} %param.24) | copy-start | bytes 196612
where the time goes:
time: 193 us
  blocking collectives  163 us (84%)
  starting transfers between devices  7.57 us (4%)
  waiting for transfers between devices  6.97 us (4%)
  other arithmetic  5.83 us (3%)
  matrix products  4.86 us (3%)
  local copies, waits for them, and re-layouts  2.97 us (2%)
    all_to_all x2, blocking collectives, sent_and_summed(): blocks = lax.all_to_all(cut_along(value, dim, size), axis, 0, 0, tiled=True)  73.7 us
    all_to_all x2, blocking collectives, sent_to_all(): return lax.all_to_all(copies, axis, split_axis=0, concat_axis=0, tiled=True)  70.3 us
    all_to_all x1, blocking collectives, summed_on_arrival(): lax.all_to_all(blocks, axis, split_axis=0, concat_axis=0, tiled=True)  19.4 us
    all_to_all x1, starting transfers between devices, sent_to_all(): return lax.all_to_all(copies, axis, split_axis=0, concat_axis=0, tiled=True)  7.57 us
    all_to_all x1, waiting for transfers between devices, sent_to_all(): return lax.all_to_all(copies, axis, split_axis=0, concat_axis=0, tiled=True)  6.97 us
  transfers between devices with their start and end apart: 1, of which 1 were waited for; matrix products, arithmetic and copies ran while one was open for 0% of the time, Pallas kernels for 0%

commit v1 on v0

v1 whole, which is shorter than its diff:
```python
import jax
import jax.numpy as jnp
import numpy as np
from jax import lax
from jax.sharding import Mesh
from jax.sharding import PartitionSpec as P

D = 2048
HEADS = 16
HEAD_DIM = 64
EPS = 1e-06
THETA = 10000.0

KV = ("y", "xh", "xl")
TP = ("b3", "b2", "b1", "b0", "c")
KAPPA = ("y", "xh")
RHO = ("xl",)
PLANES = ("b1", "b0", "c")
FAR = ("b3", "b2")


def size_of(axes):
    return int(np.prod([lax.axis_size(a) for a in axes]))


def swap(blocks, axes):
    return lax.all_to_all(blocks, axes, split_axis=0, concat_axis=0, tiled=True)


def to_all(value, axes):
    return swap(jnp.broadcast_to(value, (size_of(axes), *value.shape)), axes)


def rotate(vectors, position):
    breadth = vectors.shape[-1]
    middle = breadth // 2
    inverse = THETA ** (-jnp.arange(middle, dtype=jnp.float32) * 2.0 / breadth)
    angles = position.astype(jnp.float32)[:, None] * inverse[None, :]
    cosine = jnp.cos(angles)
    sine = jnp.sin(angles)
    former = vectors[..., :middle]
    latter = vectors[..., middle:]
    return jnp.concatenate(
        [former * cosine - latter * sine, former * sine + latter * cosine], axis=-1
    )


def on_device(
    tokens,
    lengths,
    query_weight,
    key_weight,
    value_weight,
    gate_weight,
    output_weight,
    mixer_gain,
    group_gain,
    channel_gain,
    up_weight,
    down_weight,
    memory_state,
):
    bf16, f32 = jnp.bfloat16, jnp.float32
    served, feats = tokens.shape
    kv, kappa, rho = size_of(KV), size_of(KAPPA), size_of(RHO)
    planes, far = size_of(PLANES), size_of(FAR)
    wide = feats * rho
    units = up_weight.shape[1] // rho

    up_cut = jnp.moveaxis(up_weight.reshape(feats, rho, units), 1, 0)
    down_cut = down_weight.reshape(rho, units, feats)
    first = channel_gain.astype(bf16)
    rest = channel_gain - first.astype(f32)
    second = rest.astype(bf16)
    third = (rest - second.astype(f32)).astype(bf16)
    gain_rows = jnp.concatenate(
        [first[None], second[None], third[None], jnp.zeros((5, feats), bf16)]
    )
    gain_rows = jnp.broadcast_to(gain_rows, (rho, *gain_rows.shape))
    both = jnp.concatenate(
        [up_cut.reshape(rho, -1, 128), down_cut.reshape(rho, -1, 128), gain_rows], axis=1
    )
    both = jnp.broadcast_to(both[:, None], (rho, far, *both.shape[1:]))
    both = swap(both.reshape(rho * far, *both.shape[2:]), RHO + FAR)
    half = (both.shape[1] - 8) // 2
    ups = both[:, :half].reshape(rho, far, feats, units)
    up = jnp.transpose(ups, (0, 2, 1, 3)).reshape(wide, far * units)
    downs = both[:, half : 2 * half].reshape(rho, far, units, feats)
    down = jnp.transpose(downs, (1, 2, 0, 3)).reshape(far * units, wide)
    pieces = both.reshape(rho, far, -1, feats)[:, 0, 2 * half :].astype(f32)
    gains = (pieces[:, 0] + pieces[:, 1] + pieces[:, 2]).reshape(wide)

    blocks = to_all(tokens, KV)
    whole_rows = jnp.moveaxis(blocks, 0, 1).reshape(served, kv * feats)
    widened = whole_rows.astype(f32)
    normed = (
        widened * lax.rsqrt(jnp.mean(widened * widened, axis=1, keepdims=True) + EPS) * mixer_gain
    ).astype(bf16)

    def project(weight):
        return jnp.dot(normed, weight, preferred_element_type=f32)

    queries = rotate(project(query_weight), lengths)
    keys_new = rotate(project(key_weight), lengths) * HEAD_DIM ** (-0.5)
    values_new = project(value_weight)
    gating = project(gate_weight)
    head = lax.axis_index(KV).astype(f32)
    decay = 1.0 - 2.0 ** (-5.0 - 5.0 * head / (HEADS - 1))
    new_state = decay * memory_state[:, 0] + keys_new[:, :, None] * values_new[:, None, :]
    readout = jnp.einsum("bkv,bk->bv", new_state, queries, precision=lax.Precision.HIGHEST)
    grouped = readout * lax.rsqrt(jnp.mean(readout * readout, axis=-1, keepdims=True) + EPS)
    merged = (grouped * group_gain * jax.nn.silu(gating)).astype(bf16)
    shares = jnp.dot(merged, output_weight, preferred_element_type=f32).astype(bf16)

    shares = jnp.moveaxis(shares.reshape(served, kappa, wide), 1, 0)
    shares = jnp.broadcast_to(shares[:, None], (kappa, rho, served, wide)).reshape(kv, served, wide)
    mixed_part = jnp.sum(swap(shares, KV).astype(f32), axis=0)
    at = lax.axis_index(KAPPA) * rho
    own = jnp.moveaxis(lax.dynamic_slice_in_dim(blocks, at, rho, 0), 0, 1).reshape(served, wide)
    after_wide = (own.astype(f32) + mixed_part).astype(bf16)

    rows = to_all(after_wide, PLANES).reshape(planes * served, wide)
    residual = rows.astype(f32)
    squares = jnp.sum(residual * residual, axis=1)
    scaled = (residual * gains).astype(bf16)
    raised_part = jnp.dot(scaled, up, preferred_element_type=f32).astype(bf16)
    part = planes * served // kappa
    hidden_units = far * units
    extra = jnp.zeros((kappa, 8, hidden_units), bf16)
    high = squares.astype(bf16)
    low = (squares - high.astype(f32)).astype(bf16)
    extra = extra.at[:, 0, :part].set(high.reshape(kappa, part))
    extra = extra.at[:, 1, :part].set(low.reshape(kappa, part))
    sent = jnp.concatenate([raised_part.reshape(kappa, part, hidden_units), extra], axis=1)
    arrived = jnp.sum(swap(sent, KAPPA).astype(f32), axis=0)
    raised = arrived[:part]
    totals = arrived[part, :part] + arrived[part + 1, :part]
    factor = lax.rsqrt(totals / D + EPS)
    hidden = jnp.square(jax.nn.relu(raised * factor[:, None])).astype(bf16)
    hidden = to_all(hidden, KAPPA).reshape(planes * served, hidden_units)
    lowered = jnp.dot(hidden, down, preferred_element_type=f32).astype(bf16)

    lowered = lowered.reshape(planes, served, rho, feats)
    lowered = jnp.transpose(lowered, (2, 0, 1, 3)).reshape(rho * planes, served, feats)
    lowered = jnp.sum(swap(lowered, RHO + PLANES).astype(f32), axis=0)
    mine = lax.axis_index(RHO) * feats
    after_mixer = lax.dynamic_slice_in_dim(after_wide, mine, feats, 1)
    mixed = (after_mixer.astype(f32) + lowered).astype(bf16)
    return (mixed, new_state[:, None])


def solution(mesh):
    fine = Mesh(mesh.devices.reshape(4, 2, 2, 2, 2, 2, 2, 2), KV + TP)
    return jax.shard_map(
        on_device,
        mesh=fine,
        in_specs=(
            P(TP, KV),
            P(TP),
            P(None, KV),
            P(None, KV),
            P(None, KV),
            P(None, KV),
            P(KV, None),
            P(None),
            P(KV),
            P(KV),
            P(KV, TP),
            P(TP, KV),
            P(TP, KV, None, None),
        ),
        out_specs=(P(TP, KV), P(TP, KV, None, None)),
        check_vma=False,
    )
```

time: 193 us -> 150 us (0.78)
  blocking collectives: 163 us -> 14.3 us
  waiting for transfers between devices: 6.97 us -> 67.4 us
  starting transfers between devices: 7.57 us -> 45.7 us
  local copies, waits for them, and re-layouts: 2.97 us -> 7.91 us
    all_to_all x5 -> x1, blocking collectives: 163 us -> 14.3 us  [swap(): return lax.all_to_all(blocks, axes, split_axis=0, concat_axis=0, tiled=True)]
    all_to_all x1 -> x6, waiting for transfers between devices: 6.97 us -> 67.4 us  [swap(): return lax.all_to_all(blocks, axes, split_axis=0, concat_axis=0, tiled=True)]
    all_to_all x1 -> x6, starting transfers between devices: 7.57 us -> 45.7 us  [swap(): return lax.all_to_all(blocks, axes, split_axis=0, concat_axis=0, tiled=True)]
    broadcast_in_dim x3 -> x7, local copies, waits for them, and re-layouts: 1.74 us -> 5 us  [the longest x3 3.18 us: to_all(): return swap(jnp.broadcast_to(value, (size_of(axes), *value.shape)), axes)]
  transfers between devices with their start and end apart: 1 -> 6, of which waited for: 1 -> 6; matrix products, arithmetic and copies ran while one was open for 0% -> 3% of each run, Pallas kernels for 0% -> 0%
where the time goes in v1:
time: 150 us
  waiting for transfers between devices  67.4 us (45%)
  starting transfers between devices  45.7 us (30%)
  blocking collectives  14.3 us (10%)
  local copies, waits for them, and re-layouts  7.91 us (5%)
  other arithmetic  6.62 us (4%)
  matrix products  6.56 us (4%)
    all_to_all x6, waiting for transfers between devices, swap(): return lax.all_to_all(blocks, axes, split_axis=0, concat_axis=0, tiled=True)  67.4 us
    all_to_all x6, starting transfers between devices, swap(): return lax.all_to_all(blocks, axes, split_axis=0, concat_axis=0, tiled=True)  45.7 us
    all_to_all x1, blocking collectives, swap(): return lax.all_to_all(blocks, axes, split_axis=0, concat_axis=0, tiled=True)  14.3 us
    broadcast_in_dim x3, local copies, waits for them, and re-layouts, to_all(): return swap(jnp.broadcast_to(value, (size_of(axes), *value.shape)), axes)  3.18 us
  transfers between devices with their start and end apart: 6, of which 6 were waited for; matrix products, arithmetic and copies ran while one was open for 3% of the time, Pallas kernels for 0%

profile of v1, /device:TPU:1, one launch (start us, length us, event | category | flops | bytes accessed | tf_op | source)
XLA Modules:
  0.0 149.6 jit_solution(17721144358985290433)
XLA Ops:
  0.7 1.6 %broadcast_in_dim.20 = bf16[16,64,128]{2,1,0:T(8,128)(2,1)} broadcast(bf16[64,128]{1,0:T(8,128)(2,1)} %param.17), dimensions={1,2} | broadcast | bytes 278528 | tf_op jit(solution)/shard_map/broadcast_in_dim | solution.py:31
  2.3 7.6 %all-to-all-start = ((bf16[16,64,128]{2,1,0:T(8,128)(2,1)}), bf16[16,64,128]{2,1,0:T(8,128)(2,1)S(1)}, u32[]{:S(2)}, u32[]{:S(2)}) async-start(bf16[16,64,128]{2,1,0:T(8,128)(2,1)} %broadcast_in_dim.20), calls=%async_computation | async-start | bytes 524288 | tf_op jit(solution)/shard_map/all_to_all | solution.py:27
  9.9 0.7 convert_element_type.141
  10.6 0.1 pad.17.clone
  10.7 0.7 convert_bitcast_fusion.4
  11.4 6.1 %all-to-all-done = bf16[16,64,128]{2,1,0:T(8,128)(2,1)S(1)} async-done(((bf16[16,64,128]{2,1,0:T(8,128)(2,1)}), bf16[16,64,128]{2,1,0:T(8,128)(2,1)S(1)}, u32[]{:S(2)}, u32[]{:S(2)}) %all-to-all-start) | async-done | bytes 262176 | tf_op jit(solution)/shard_map/all_to_all | solution.py:27
  17.6 0.2 fusion.8
  17.7 0.8 fusion.10
  18.6 1.2 fusion.42
  19.8 0.2 fusion.43
  20.0 1.2 fusion.41
  21.2 0.2 fusion.27
  21.4 0.1 copy.49
  21.5 0.1 copy.57
  21.6 2.2 %fusion = f32[64,1,64]{2,1,0:T(1,128)S(1)} fusion(f32[64,64,1]{1,2,0:T(1,128)S(1)} %copy.57, f32[64,1,64,64]{3,2,1,0:T(8,128)S(1)} %copy-done.1, f32[64,64]{1,0:T(8,128)S(1)} %fusion.42, f32[64,64]{1,0:T(8,128)S(1)} %copy.49, f32[]{:T(128)S(6)} %sub.29), kind=kOutput, calls=%fused_computation.2 | convolution fusion | flops 3932160 | bytes 1114116 | tf_op jit(solution)/shard_map/bkv,bk->bv/dot_general | solution.py:110
  23.7 0.1 multiply_reduce_fusion
  23.9 0.5 convolution_convert_fusion
  24.4 0.1 copy.62
  24.5 0.9 broadcast_in_dim.21
  25.4 3.6 %all-to-all-start.1 = ((bf16[16,64,256]{2,1,0:T(8,128)(2,1)}), bf16[16,64,256]{2,1,0:T(8,128)(2,1)S(1)}, u32[]{:S(2)}, u32[]{:S(2)}) async-start(bf16[16,64,256]{2,1,0:T(8,128)(2,1)} %bitcast.95), calls=%async_computation.1 | async-start | bytes 1048576 | tf_op jit(solution)/shard_map/all_to_all | solution.py:27
  29.0 0.1 maximum_maximum_fusion
  29.1 9.1 %all-to-all-done.1 = bf16[16,64,256]{2,1,0:T(8,128)(2,1)S(1)} async-done(((bf16[16,64,256]{2,1,0:T(8,128)(2,1)}), bf16[16,64,256]{2,1,0:T(8,128)(2,1)S(1)}, u32[]{:S(2)}, u32[]{:S(2)}) %all-to-all-start.1) | async-done | bytes 524320 | tf_op jit(solution)/shard_map/all_to_all | solution.py:27
  38.2 1.0 broadcast_in_dim.28
  39.2 0.1 copy-done.2
  39.2 15.2 %all-to-all-start.3 = ((bf16[8,264,128]{2,1,0:T(8,128)(2,1)}), bf16[8,264,128]{2,1,0:T(8,128)(2,1)S(1)}, u32[]{:S(2)}, u32[]{:S(2)}) async-start(bf16[8,264,128]{2,1,0:T(8,128)(2,1)} %bitcast.13), calls=%async_computation.3 | async-start | bytes 1081344 | tf_op jit(solution)/shard_map/all_to_all | solution.py:27
  54.4 1.1 convert_reduce_fusion.1
  55.6 26.6 %all-to-all-done.3 = bf16[8,264,128]{2,1,0:T(8,128)(2,1)S(1)} async-done(((bf16[8,264,128]{2,1,0:T(8,128)(2,1)}), bf16[8,264,128]{2,1,0:T(8,128)(2,1)S(1)}, u32[]{:S(2)}, u32[]{:S(2)}) %all-to-all-start.3) | async-done | bytes 540704 | tf_op jit(solution)/shard_map/all_to_all | solution.py:27
  82.1 0.7 broadcast_in_dim.22
  82.8 7.6 %all-to-all-start.2 = ((bf16[8,64,256]{2,1,0:T(8,128)(2,1)}), bf16[8,64,256]{2,1,0:T(8,128)(2,1)S(1)}, u32[]{:S(2)}, u32[]{:S(2)}) async-start(bf16[8,64,256]{2,1,0:T(8,128)(2,1)} %broadcast_in_dim.22), calls=%async_computation.2 | async-start | bytes 524288 | tf_op jit(solution)/shard_map/all_to_all | solution.py:27
  90.4 8.7 %all-to-all-done.2 = bf16[8,64,256]{2,1,0:T(8,128)(2,1)S(1)} async-done(((bf16[8,64,256]{2,1,0:T(8,128)(2,1)}), bf16[8,64,256]{2,1,0:T(8,128)(2,1)S(1)}, u32[]{:S(2)}, u32[]{:S(2)}) %all-to-all-start.2) | async-done | bytes 262176 | tf_op jit(solution)/shard_map/all_to_all | solution.py:27
  99.1 0.1 fusion.6
  99.3 0.2 scatter.9
  99.5 0.2 copy.52
  99.7 0.3 convolution_convert_fusion.1
  100.1 14.3 %all_to_all.35 = bf16[8,72,512]{2,1,0:T(8,128)(2,1)S(1)} all-to-all(bf16[8,72,512]{2,1,0:T(8,128)(2,1)S(1)} %pad_maximum_fusion), channel_id=1, replica_groups=mesh['y'=4,'xh'=2,'xl'=2,'b3'=2,'b2'=2,'b1'=2,'b0'=2,'c'=2] {'y','xh'}, dimensions={0} | all-to-all | bytes 1179648 | tf_op jit(solution)/shard_map/all_to_all | solution.py:27
  114.4 0.1 convert_reduce_fusion
  114.5 0.1 fusion.17
  114.6 0.8 broadcast_in_dim.58
  115.5 3.5 %all-to-all-start.5 = ((bf16[8,64,512]{2,1,0:T(8,128)(2,1)}), bf16[8,64,512]{2,1,0:T(8,128)(2,1)S(1)}, u32[]{:S(2)}, u32[]{:S(2)}) async-start(bf16[8,64,512]{2,1,0:T(8,128)(2,1)} %broadcast_in_dim.58), calls=%async_computation.5 | async-start | bytes 1048576 | tf_op jit(solution)/shard_map/all_to_all | solution.py:27
  119.0 0.3 copy.54
  119.2 9.1 %all-to-all-done.5 = bf16[8,64,512]{2,1,0:T(8,128)(2,1)S(1)} async-done(((bf16[8,64,512]{2,1,0:T(8,128)(2,1)}), bf16[8,64,512]{2,1,0:T(8,128)(2,1)S(1)}, u32[]{:S(2)}, u32[]{:S(2)}) %all-to-all-start.5) | async-done | bytes 524320 | tf_op jit(solution)/shard_map/all_to_all | solution.py:27
  128.3 1.0 convolution_convert_fusion.2
  129.3 1.0 reshape.252
  130.3 0.8 copy.55
  131.1 8.3 %all-to-all-start.6 = ((bf16[16,64,128]{2,1,0:T(8,128)(2,1)}), bf16[16,64,128]{2,1,0:T(8,128)(2,1)S(1)}, u32[]{:S(2)}, u32[]{:S(2)}) async-start(bf16[16,64,128]{2,1,0:T(8,128)(2,1)} %bitcast.28), calls=%async_computation.6 | async-start | bytes 524288 | tf_op jit(solution)/shard_map/all_to_all | solution.py:27
  139.4 1.7 %multiply_add_fusion = f32[64,1,64,64]{3,2,1,0:T(8,128)} fusion(f32[64,1,64,64]{3,2,1,0:T(8,128)S(1)} %copy-done.1, f32[64,64]{1,0:T(8,128)S(1)} %fusion.42, f32[64,64]{1,0:T(8,128)S(1)} %copy.49, f32[]{:T(128)S(6)} %sub.29), kind=kLoop, calls=%fused_computation.3 | loop fusion | flops 786432 | bytes 2129924 | tf_op jit(solution)/shard_map/add | solution.py:109
  141.1 7.8 %all-to-all-done.6 = bf16[16,64,128]{2,1,0:T(8,128)(2,1)S(1)} async-done(((bf16[16,64,128]{2,1,0:T(8,128)(2,1)}), bf16[16,64,128]{2,1,0:T(8,128)(2,1)S(1)}, u32[]{:S(2)}, u32[]{:S(2)}) %all-to-all-start.6) | async-done | bytes 262176 | tf_op jit(solution)/shard_map/all_to_all | solution.py:27
  149.0 0.6 add_convert_fusion
  (35 shorter events, 0.4 us)
Async XLA Ops:
  0.6 23.2 %copy-start = (bf16[64,2048]{1,0:T(8,128)(2,1)S(1)}, bf16[64,2048]{1,0:T(8,128)(2,1)}, u32[]{:S(2)}) copy-start(bf16[64,2048]{1,0:T(8,128)(2,1)} %param.23) | copy-start | bytes 786436
  0.6 19.2 %copy-start.4 = (bf16[2048,64]{0,1:T(8,128)(2,1)S(1)}, bf16[2048,64]{0,1:T(8,128)(2,1)}, u32[]{:S(2)}) copy-start(bf16[2048,64]{0,1:T(8,128)(2,1)} %param.19) | copy-start | bytes 786436
  0.7 20.9 %copy-start.1 = (f32[64,1,64,64]{3,2,1,0:T(8,128)S(1)}, f32[64,1,64,64]{3,2,1,0:T(8,128)}, u32[]{:S(2)}) copy-start(f32[64,1,64,64]{3,2,1,0:T(8,128)} %param.29) | copy-start | bytes 3145732
  2.3 15.3 %all-to-all-start = ((bf16[16,64,128]{2,1,0:T(8,128)(2,1)}), bf16[16,64,128]{2,1,0:T(8,128)(2,1)S(1)}, u32[]{:S(2)}, u32[]{:S(2)}) async-start(bf16[16,64,128]{2,1,0:T(8,128)(2,1)} %broadcast_in_dim.20), calls=%async_computation | async-start | bytes 524288 | tf_op jit(solution)/shard_map/all_to_all | solution.py:27
  18.6 5.3 %copy-start.3 = (bf16[2048,64]{0,1:T(8,128)(2,1)S(1)}, bf16[2048,64]{0,1:T(8,128)(2,1)}, u32[]{:S(2)}) copy-start(bf16[2048,64]{0,1:T(8,128)(2,1)} %param.22) | copy-start | bytes 786436
  18.6 5.3 %copy-start.7 = (f32[64]{0:T(128)S(1)}, f32[64]{0:T(128)}, u32[]{:S(2)}) copy-start(f32[64]{0:T(128)} %param.25) | copy-start | bytes 772
  24.4 4.7 %copy-start.5 = (bf16[128,256]{1,0:T(8,128)(2,1)S(1)}, bf16[128,256]{1,0:T(8,128)(2,1)}, u32[]{:S(2)}) copy-start(bf16[128,256]{1,0:T(8,128)(2,1)} %param.27) | copy-start | bytes 196612
  24.4 4.7 %copy-start.6 = (bf16[256,128]{1,0:T(8,128)(2,1)S(1)}, bf16[256,128]{1,0:T(8,128)(2,1)}, u32[]{:S(2)}) copy-start(bf16[256,128]{1,0:T(8,128)(2,1)} %param.28) | copy-start | bytes 196612
  25.4 12.8 %all-to-all-start.1 = ((bf16[16,64,256]{2,1,0:T(8,128)(2,1)}), bf16[16,64,256]{2,1,0:T(8,128)(2,1)S(1)}, u32[]{:S(2)}, u32[]{:S(2)}) async-start(bf16[16,64,256]{2,1,0:T(8,128)(2,1)} %bitcast.95), calls=%async_computation.1 | async-start | bytes 1048576 | tf_op jit(solution)/shard_map/all_to_all | solution.py:27
  38.2 1.0 copy-start.2
  39.2 42.9 %all-to-all-start.3 = ((bf16[8,264,128]{2,1,0:T(8,128)(2,1)}), bf16[8,264,128]{2,1,0:T(8,128)(2,1)S(1)}, u32[]{:S(2)}, u32[]{:S(2)}) async-start(bf16[8,264,128]{2,1,0:T(8,128)(2,1)} %bitcast.13), calls=%async_computation.3 | async-start | bytes 1081344 | tf_op jit(solution)/shard_map/all_to_all | solution.py:27
  82.8 16.2 %all-to-all-start.2 = ((bf16[8,64,256]{2,1,0:T(8,128)(2,1)}), bf16[8,64,256]{2,1,0:T(8,128)(2,1)S(1)}, u32[]{:S(2)}, u32[]{:S(2)}) async-start(bf16[8,64,256]{2,1,0:T(8,128)(2,1)} %broadcast_in_dim.22), calls=%async_computation.2 | async-start | bytes 524288 | tf_op jit(solution)/shard_map/all_to_all | solution.py:27
  115.5 12.9 %all-to-all-start.5 = ((bf16[8,64,512]{2,1,0:T(8,128)(2,1)}), bf16[8,64,512]{2,1,0:T(8,128)(2,1)S(1)}, u32[]{:S(2)}, u32[]{:S(2)}) async-start(bf16[8,64,512]{2,1,0:T(8,128)(2,1)} %broadcast_in_dim.58), calls=%async_computation.5 | async-start | bytes 1048576 | tf_op jit(solution)/shard_map/all_to_all | solution.py:27
  131.1 17.8 %all-to-all-start.6 = ((bf16[16,64,128]{2,1,0:T(8,128)(2,1)}), bf16[16,64,128]{2,1,0:T(8,128)(2,1)S(1)}, u32[]{:S(2)}, u32[]{:S(2)}) async-start(bf16[16,64,128]{2,1,0:T(8,128)(2,1)} %bitcast.28), calls=%async_computation.6 | async-start | bytes 524288 | tf_op jit(solution)/shard_map/all_to_all | solution.py:27
